TPU v7x, 32 devices: a whole 2x2x4 slice. The times are simulated.
32 devices in a mesh: ep: 8 (over z, core), tp: 4 (over y, x).
Axes of the slice: x: 2, y: 2, z: 4, core: 2. Of those that a mesh axis runs over, the one named last changes fastest.
Arguments:
- tokens: bfloat16 [2048, 2048], P('ep'), may hold values from -6 to 6
- gate_proj: bfloat16 [8, 2048, 4096], P('ep', None, 'tp'), may hold values from -0.125 to 0.125
- up_proj: bfloat16 [8, 2048, 4096], P('ep', None, 'tp'), may hold values from -0.125 to 0.125
- down_proj: bfloat16 [8, 4096, 2048], P('ep', 'tp'), may hold values from -0.09375 to 0.09375
- side_input_weight: bfloat16 [2048, 1024], P(None, 'tp'), may hold values from -0.125 to 0.125
- dense_out: bfloat16 [1024, 2048], P(None, 'tp'), may hold values from -0.1875 to 0.1875
- dense_gate: bfloat16 [2048], replicated, may hold values from -0.125 to 0.125
- chosen_rows: int32 [8, 256], P(None, 'ep'), may hold values from 0 to 255, as said below
- choice_weights: float32 [8, 256], P(None, 'ep'), may hold values from 0.25 to 1
Outputs:
- mixed: bfloat16 [2048, 2048], P('ep', 'tp')
Inputs may be any that keep to these rules, and one draw needn't show every extreme that they name: `chosen_rows`: for each expert and each block of 32 columns (one index of ep), the 32 rows are distinct rows of that index's 256 tokens; every expert reads exactly 32 tokens of every index.
All inputs are finite; a program needn't handle non-finite values.
Results may differ from a plain program's by a relative error of at most 0.015.
Values may be sent and summed in bfloat16 or wider, within the bound.
No kernel may reach another device: no remote copies, remote signals or barrier semaphores. Data moves between devices by JAX's collectives and lax.ppermute only.
A program may use at most 64 MiB of HBM per device.

v0:
```python
import jax
import jax.numpy as jnp
from jax import lax
from jax.sharding import PartitionSpec as P


def per_device(
    tokens,
    gate_proj,
    up_proj,
    down_proj,
    side_input_weight,
    dense_out,
    dense_gate,
    chosen_rows,
    choice_weights,
):
    tok_rows = tokens.shape[0]
    width = tokens.shape[1] // lax.axis_size("tp")
    column_position = lax.axis_index("tp") * width
    own_cols = lax.dynamic_slice_in_dim(tokens, column_position, width, 1)
    expert_count, slot_rows = chosen_rows.shape
    capacity = expert_count * slot_rows
    picked = jnp.take(own_cols, chosen_rows.reshape(-1), axis=0).reshape(
        expert_count, slot_rows, width
    )
    arrived = lax.all_to_all(picked, "ep", split_axis=0, concat_axis=1, tiled=True).reshape(
        capacity, width
    )
    w_gate = gate_proj[0]
    w_up = up_proj[0]
    w_down = down_proj[0]
    piece = lax.all_gather(arrived, "tp", axis=1, tiled=True)
    gate_val = jnp.dot(piece, w_gate, preferred_element_type=jnp.float32)
    up_val = jnp.dot(piece, w_up, preferred_element_type=jnp.float32)
    hidden = (jax.nn.silu(gate_val) * up_val).astype(jnp.bfloat16)
    summed = lax.psum_scatter(
        lax.dot_general(
            w_down, hidden, (((0,), (1,)), ((), ())), preferred_element_type=jnp.float32
        ).astype(jnp.bfloat16),
        "tp",
        scatter_dimension=0,
        tiled=True,
    )
    returned = lax.all_to_all(summed, "ep", split_axis=1, concat_axis=1, tiled=True)
    hits = (
        chosen_rows.reshape(-1)[:, None] == jnp.arange(tok_rows, dtype=jnp.int32)[None, :]
    ).astype(jnp.bfloat16)
    scaled = returned.astype(jnp.float32) * choice_weights.reshape(-1)[None, :]
    high_part = scaled.astype(jnp.bfloat16)
    lower_half = (scaled - high_part.astype(jnp.float32)).astype(jnp.bfloat16)
    contract = (((0,), (1,)), ((), ()))
    routed = lax.dot_general(
        hits, high_part, contract, preferred_element_type=jnp.float32
    ) + lax.dot_general(hits, lower_half, contract, preferred_element_type=jnp.float32)
    dense_hidden = jax.nn.silu(
        jnp.dot(tokens, side_input_weight, preferred_element_type=jnp.float32)
    ).astype(jnp.bfloat16)
    dense_val = jnp.dot(
        lax.all_gather(dense_hidden, "tp", axis=1, tiled=True),
        dense_out,
        preferred_element_type=jnp.float32,
    )
    side_gate = jax.nn.sigmoid(jnp.dot(tokens, dense_gate, preferred_element_type=jnp.float32))
    return (routed + side_gate[:, None] * dense_val).astype(jnp.bfloat16)


def solution(mesh):
    placed = (
        P("ep", None),
        P("ep", None, "tp"),
        P("ep", None, "tp"),
        P("ep", "tp", None),
        P(None, "tp"),
        P(None, "tp"),
        P(),
        P(None, "ep"),
        P(None, "ep"),
    )
    return jax.shard_map(
        per_device, mesh=mesh, in_specs=placed, out_specs=P("ep", "tp"), check_vma=False
    )
```

profile of v0, /device:TPU:0, one launch (start us, length us, event | category | flops | bytes accessed | tf_op | source)
XLA Modules:
  0.0 116.5 jit_solution(18036005292770435474)
XLA Ops:
  6.5 0.0 copy-start
  6.5 0.0 all-gather.2.cloned.1.call-start
  6.5 0.9 reshape.57
  7.4 0.7 compare_and_fusion
  8.1 0.0 copy-done
  8.1 1.2 gather_fusion
  9.3 0.1 broadcast_select_fusion
  9.4 16.0 %all_to_all.18 = bf16[8,32,512]{2,1,0:T(8,128)(2,1)} all-to-all(bf16[8,32,512]{2,1,0:T(8,128)(2,1)S(1)} %broadcast_select_fusion), channel_id=1, replica_groups=mesh['ep'=8,'tp'=4] {'ep'}, dimensions={0} | all-to-all | bytes 524288 | tf_op jit(solution)/shard_map/all_to_all | solution.py:27
  25.4 0.0 all-gather.2.cloned.1.call-update
  25.4 0.0 reduce-scatter.2.cloned.1.call-start
  25.4 25.4 %all-gather.2.cloned.1.call-done = bf16[256,2048]{1,0:T(8,128)(2,1)} async-done(((bf16[256,512]{1,0:T(8,128)(2,1)}), bf16[256,2048]{1,0:T(8,128)(2,1)}) %all-gather.2.cloned.1.call-update) | async-done | bytes 1048592 | tf_op jit(solution)/shard_map/all_gather | solution.py:33
  50.9 0.0 copy-start.5
  50.9 3.8 %fusion.4 = f32[256,1024]{1,0:T(8,128)S(1)} fusion(bf16[256,2048]{1,0:T(8,128)(2,1)} %all-gather.2.cloned.1.call-done, bf16[1,2048,1024]{2,1,0:T(8,128)(2,1)} %param.10), kind=kOutput, calls=%fused_computation.5 | convolution fusion | flops 1073741824 | bytes 6291456 | tf_op jit(solution)/shard_map/dot_general | solution.py:34
  54.7 0.0 copy-done.5
  54.7 0.0 copy-start.2
  54.7 0.0 copy-start.4
  54.7 0.0 copy-start.3
  54.7 6.9 %fusion.9 = bf16[2048,256]{0,1:T(8,128)(2,1)} fusion(bf16[1,1024,2048]{2,1,0:T(8,128)(2,1)} %param.12, bf16[256,2048]{1,0:T(8,128)(2,1)S(1)} %copy-done.5, bf16[1,2048,1024]{2,1,0:T(8,128)(2,1)} %param.11, f32[256,1024]{1,0:T(8,128)S(1)} %fusion.4), kind=kOutput, calls=%fused_computation.8 | convolution fusion | flops 2149580800 | bytes 11534336 | tf_op jit(solution)/shard_map/dot_general | solution.py:38
  61.7 0.0 reduce-scatter.2.cloned.1.call-update
  61.7 0.0 copy-done.2
  61.7 0.1 eq.15
  61.8 0.0 copy-done.4
  61.8 0.1 mul.35
  61.8 0.0 copy-done.3
  61.9 0.0 copy-start.1
  61.9 1.8 %multiply_convert_fusion = bf16[256,256]{1,0:T(8,128)(2,1)S(1)} fusion(bf16[256,2048]{1,0:T(8,128)(2,1)S(1)} %copy-done, bf16[2048,256]{1,0:T(8,128)(2,1)} %param.13), kind=kOutput, calls=%fused_computation.20 | convolution fusion | flops 268763136 | bytes 2228224 | tf_op jit(solution)/shard_map/dot_general | solution.py:57
  63.6 17.9 %all_gather.7 = bf16[256,1024]{1,0:T(8,128)(2,1)S(1)} all-gather(bf16[256,256]{1,0:T(8,128)(2,1)S(1)} %multiply_convert_fusion), channel_id=1, replica_groups=mesh['ep'=8,'tp'=4] {'tp'}, dimensions={1}, use_global_device_ids=true | all-gather | bytes 655360 | tf_op jit(solution)/shard_map/all_gather | solution.py:60
  81.6 11.8 %reduce-scatter.2.cloned.1.call-done = bf16[512,256]{0,1:T(8,128)(2,1)} async-done(((bf16[2048,256]{0,1:T(8,128)(2,1)}), bf16[512,256]{0,1:T(8,128)(2,1)}) %reduce-scatter.2.cloned.1.call-update) | async-done | bytes 262160 | tf_op jit(solution)/shard_map/reduce_scatter | solution.py:37
  93.3 4.6 %all-to-all-start.1 = ((bf16[512,8,32]{0,2,1:T(8,128)(2,1)}), bf16[512,8,32]{0,2,1:T(8,128)(2,1)S(1)}, u32[]{:S(2)}, u32[]{:S(2)}) async-start(bf16[512,8,32]{0,2,1:T(8,128)(2,1)} %bitcast.41), calls=%async_computation.2 | async-start | bytes 524288 | tf_op jit(solution)/shard_map/all_to_all | solution.py:45
  97.9 0.4 fusion.32
  98.3 9.3 %all-to-all-done.1 = bf16[512,8,32]{0,2,1:T(8,128)(2,1)S(1)} async-done(((bf16[512,8,32]{0,2,1:T(8,128)(2,1)}), bf16[512,8,32]{0,2,1:T(8,128)(2,1)S(1)}, u32[]{:S(2)}, u32[]{:S(2)}) %all-to-all-start.1) | async-done | bytes 262176 | tf_op jit(solution)/shard_map/all_to_all | solution.py:45
  107.7 0.1 fusion.23
  107.8 0.3 fusion.28
  108.1 0.4 convolution_add_fusion
  108.5 0.0 copy-done.1
  108.5 1.1 fusion.19
  (5 shorter events, 0.1 us)
Async XLA Ops:
  6.5 1.6 %copy-start = (bf16[256,2048]{1,0:T(8,128)(2,1)S(1)}, bf16[256,2048]{1,0:T(8,128)(2,1)}, u32[]{:S(2)}) copy-start(bf16[256,2048]{1,0:T(8,128)(2,1)} %param.9) | copy-start | bytes 3145732
  6.5 44.3 %all-gather.2.cloned.1.call-start = ((), (), s32[]{:S(2)}) async-start(), calls=%async_computation.3 | async-start | bytes 1310720 | tf_op jit(solution)/shard_map/all_gather | solution.py:33
  25.4 67.9 %reduce-scatter.2.cloned.1.call-start = ((), (), s32[]{:S(2)}) async-start(), calls=%async_computation.4 | async-start | bytes 1310720 | tf_op jit(solution)/shard_map/reduce_scatter | solution.py:37
  50.9 3.8 %copy-start.5 = (bf16[256,2048]{1,0:T(8,128)(2,1)S(1)}, bf16[256,2048]{1,0:T(8,128)(2,1)}, u32[]{:S(2)}) copy-start(bf16[256,2048]{1,0:T(8,128)(2,1)} %all-gather.2.cloned.1.call-done) | copy-start | bytes 3145732
  54.7 7.0 %copy-start.2 = (s32[8,32]{1,0:T(8,128)S(1)}, s32[8,32]{1,0:T(8,128)}, u32[]{:S(2)}) copy-start(s32[8,32]{1,0:T(8,128)} %param.16) | copy-start | bytes 3076
  54.7 7.0 %copy-start.4 = (f32[8,32]{1,0:T(8,128)S(1)}, f32[8,32]{1,0:T(8,128)}, u32[]{:S(2)}) copy-start(f32[8,32]{1,0:T(8,128)} %param.17) | copy-start | bytes 3076
  54.7 7.1 %copy-start.3 = (bf16[2048]{0:T(1024)(128)(2,1)S(1)}, bf16[2048]{0:T(1024)(128)(2,1)}, u32[]{:S(2)}) copy-start(bf16[2048]{0:T(1024)(128)(2,1)} %param.15) | copy-start | bytes 12292
  61.9 46.7 %copy-start.1 = (bf16[1024,512]{1,0:T(8,128)(2,1)S(1)}, bf16[1024,512]{1,0:T(8,128)(2,1)}, u32[]{:S(2)}) copy-start(bf16[1024,512]{1,0:T(8,128)(2,1)} %param.14) | copy-start | bytes 3145732
  93.3 14.3 %all-to-all-start.1 = ((bf16[512,8,32]{0,2,1:T(8,128)(2,1)}), bf16[512,8,32]{0,2,1:T(8,128)(2,1)S(1)}, u32[]{:S(2)}, u32[]{:S(2)}) async-start(bf16[512,8,32]{0,2,1:T(8,128)(2,1)} %bitcast.41), calls=%async_computation.2 | async-start | bytes 524288 | tf_op jit(solution)/shard_map/all_to_all | solution.py:45
Sparse Core Ops, SparseCore 0:
  25.5 25.2 all-gather.1
  61.8 31.4 reduce-scatter.1
where the time goes:
time: 117 us
  waiting for transfers between devices  46.5 us (40%)
  blocking collectives  33.9 us (29%)
  matrix products  14.8 us (13%)
  between operations  13.5 us (12%)
  starting transfers between devices  4.65 us (4%)
  local copies, waits for them, and re-layouts  2.23 us (2%)
    all_gather x1, waiting for transfers between devices, per_device(): piece = lax.all_gather(arrived, 'tp', axis=1, tiled=True)  25.4 us
    all_gather x1, blocking collectives, per_device(): lax.all_gather(dense_hidden, 'tp', axis=1, tiled=True)  17.9 us
    all_to_all x1, blocking collectives, per_device(): lax.all_to_all(picked, 'ep', split_axis=0, concat_axis=1, tiled=True)  16 us
    reduce_scatter x1, waiting for transfers between devices, per_device(): lax.psum_scatter(lax.dot_general(w_down, hidden, (((0,), (1,)), ((), ()))...  11.8 us
    all_to_all x1, waiting for transfers between devices, per_device(): lax.all_to_all(summed, 'ep', split_axis=1, concat_axis=1, tiled=True)  9.33 us
    dot_general x1, matrix products, per_device(): lax.dot_general(w_down, hidden, (((0,), (1,)), ((), ())), preferred_eleme...  6.9 us
    all_to_all x1, starting transfers between devices, per_device(): lax.all_to_all(summed, 'ep', split_axis=1, concat_axis=1, tiled=True)  4.61 us
    dot_general x1, matrix products, per_device(): gate_val = jnp.dot(piece, w_gate, preferred_element_type=jnp.float32)  3.83 us
  transfers between devices with their start and end apart: 3, of which 3 were waited for; matrix products, arithmetic and copies ran while one was open for 2% of the time, Pallas kernels for 0%

commit v1 on v0

--- a/solution.py
+++ b/solution.py
@@ -30,7 +30,8 @@
     w_gate = gate_proj[0]
     w_up = up_proj[0]
     w_down = down_proj[0]
-    piece = lax.all_gather(arrived, "tp", axis=1, tiled=True)
+    parts = lax.all_gather(arrived, "tp", axis=0, tiled=False)
+    piece = jnp.concatenate(parts, axis=1)
     gate_val = jnp.dot(piece, w_gate, preferred_element_type=jnp.float32)
     up_val = jnp.dot(piece, w_up, preferred_element_type=jnp.float32)
     hidden = (jax.nn.silu(gate_val) * up_val).astype(jnp.bfloat16)

time: 117 us -> 118 us (level)
  local copies, waits for them, and re-layouts: 2.23 us -> 3.7 us
    all_gather x0 -> x1, local copies, waits for them, and re-layouts: none -> 1.47 us  [per_device(): parts = lax.all_gather(arrived, 'tp', axis=0, tiled=False)]
where the time goes in v1:
time: 118 us
  waiting for transfers between devices  46.7 us (40%)
  blocking collectives  33.9 us (29%)
  matrix products  14.4 us (12%)
  between operations  13.5 us (11%)
  starting transfers between devices  4.66 us (4%)
  local copies, waits for them, and re-layouts  3.7 us (3%)
    all_gather x1, waiting for transfers between devices, per_device(): parts = lax.all_gather(arrived, 'tp', axis=0, tiled=False)  25.5 us
    all_gather x1, blocking collectives, per_device(): lax.all_gather(dense_hidden, 'tp', axis=1, tiled=True)  17.9 us
    all_to_all x1, blocking collectives, per_device(): lax.all_to_all(picked, 'ep', split_axis=0, concat_axis=1, tiled=True)  16 us
    reduce_scatter x1, waiting for transfers between devices, per_device(): lax.psum_scatter(lax.dot_general(w_down, hidden, (((0,), (1,)), ((), ()))...  11.8 us
    all_to_all x1, waiting for transfers between devices, per_device(): lax.all_to_all(summed, 'ep', split_axis=1, concat_axis=1, tiled=True)  9.33 us
    dot_general x1, matrix products, per_device(): lax.dot_general(w_down, hidden, (((0,), (1,)), ((), ())), preferred_eleme...  6.93 us
    all_to_all x1, starting transfers between devices, per_device(): lax.all_to_all(summed, 'ep', split_axis=1, concat_axis=1, tiled=True)  4.61 us
    dot_general x1, matrix products, per_device(): gate_val = jnp.dot(piece, w_gate, preferred_element_type=jnp.float32)  3.46 us
  transfers between devices with their start and end apart: 3, of which 3 were waited for; matrix products, arithmetic and copies ran while one was open for 2% of the time, Pallas kernels for 0%

profile of v1, /device:TPU:0, one launch (start us, length us, event | category | flops | bytes accessed | tf_op | source)
XLA Modules:
  0.0 117.8 jit_solution(2439496366504698470)
XLA Ops:
  6.5 0.0 copy-start
  6.5 0.0 all-gather.2.cloned.1.call-start
  6.5 0.9 reshape.59
  7.4 0.7 compare_and_fusion
  8.1 0.0 copy-done
  8.1 1.2 gather_fusion
  9.3 0.1 broadcast_select_fusion
  9.4 16.0 %all_to_all.21 = bf16[8,32,512]{2,1,0:T(8,128)(2,1)} all-to-all(bf16[8,32,512]{2,1,0:T(8,128)(2,1)S(1)} %broadcast_select_fusion), channel_id=1, replica_groups=mesh['ep'=8,'tp'=4] {'ep'}, dimensions={0} | all-to-all | bytes 524288 | tf_op jit(solution)/shard_map/all_to_all | solution.py:27
  25.4 0.0 all-gather.2.cloned.1.call-update
  25.4 0.0 reduce-scatter.2.cloned.1.call-start
  25.4 25.5 %all-gather.2.cloned.1.call-done = bf16[4,256,512]{2,1,0:T(8,128)(2,1)} async-done(((bf16[1,256,512]{2,1,0:T(8,128)(2,1)}), bf16[4,256,512]{2,1,0:T(8,128)(2,1)}) %all-gather.2.cloned.1.call-update) | async-done | bytes 1048592 | tf_op jit(solution)/shard_map/all_gather | solution.py:33
  51.0 1.5 %copy.12 = bf16[4,256,512]{1,2,0:T(8,128)(2,1)S(1)} copy(bf16[4,256,512]{2,1,0:T(8,128)(2,1)} %all-gather.2.cloned.1.call-done) | data formatting | bytes 2097152 | tf_op jit(solution)/shard_map/all_gather | solution.py:33
  52.5 3.5 %fusion.4 = f32[256,1024]{1,0:T(8,128)S(1)} fusion(bf16[256,2048]{0,1:T(8,128)(2,1)S(1)} %bitcast.43, bf16[1,2048,1024]{2,1,0:T(8,128)(2,1)} %param.10), kind=kOutput, calls=%fused_computation.5 | convolution fusion | flops 1073741824 | bytes 6291456 | tf_op jit(solution)/shard_map/dot_general | solution.py:35
  55.9 0.0 copy-start.2
  55.9 0.0 copy-start.4
  56.0 0.0 copy-start.3
  56.0 6.9 %fusion.9 = bf16[2048,256]{0,1:T(8,128)(2,1)} fusion(bf16[1,1024,2048]{2,1,0:T(8,128)(2,1)} %param.12, bf16[256,2048]{0,1:T(8,128)(2,1)S(1)} %bitcast.44, bf16[1,2048,1024]{2,1,0:T(8,128)(2,1)} %param.11, f32[256,1024]{1,0:T(8,128)S(1)} %fusion.4), kind=kOutput, calls=%fused_computation.8 | convolution fusion | flops 2149580800 | bytes 11534336 | tf_op jit(solution)/shard_map/dot_general | solution.py:39
  62.9 0.0 reduce-scatter.2.cloned.1.call-update
  62.9 0.0 copy-done.2
  62.9 0.1 eq.15
  63.0 0.0 copy-done.4
  63.0 0.1 mul.35
  63.1 0.0 copy-done.3
  63.1 0.0 copy-start.1
  63.1 1.8 %multiply_convert_fusion = bf16[256,256]{1,0:T(8,128)(2,1)S(1)} fusion(bf16[256,2048]{1,0:T(8,128)(2,1)S(1)} %copy-done, bf16[2048,256]{1,0:T(8,128)(2,1)} %param.13), kind=kOutput, calls=%fused_computation.20 | convolution fusion | flops 268763136 | bytes 2228224 | tf_op jit(solution)/shard_map/dot_general | solution.py:58
  64.9 17.9 %all_gather.7 = bf16[256,1024]{1,0:T(8,128)(2,1)S(1)} all-gather(bf16[256,256]{1,0:T(8,128)(2,1)S(1)} %multiply_convert_fusion), channel_id=1, replica_groups=mesh['ep'=8,'tp'=4] {'tp'}, dimensions={1}, use_global_device_ids=true | all-gather | bytes 655360 | tf_op jit(solution)/shard_map/all_gather | solution.py:61
  82.8 11.8 %reduce-scatter.2.cloned.1.call-done = bf16[512,256]{0,1:T(8,128)(2,1)} async-done(((bf16[2048,256]{0,1:T(8,128)(2,1)}), bf16[512,256]{0,1:T(8,128)(2,1)}) %reduce-scatter.2.cloned.1.call-update) | async-done | bytes 262160 | tf_op jit(solution)/shard_map/reduce_scatter | solution.py:38
  94.6 4.6 %all-to-all-start.1 = ((bf16[512,8,32]{0,2,1:T(8,128)(2,1)}), bf16[512,8,32]{0,2,1:T(8,128)(2,1)S(1)}, u32[]{:S(2)}, u32[]{:S(2)}) async-start(bf16[512,8,32]{0,2,1:T(8,128)(2,1)} %bitcast.46), calls=%async_computation.2 | async-start | bytes 524288 | tf_op jit(solution)/shard_map/all_to_all | solution.py:46
  99.2 0.4 fusion.32
  99.6 9.3 %all-to-all-done.1 = bf16[512,8,32]{0,2,1:T(8,128)(2,1)S(1)} async-done(((bf16[512,8,32]{0,2,1:T(8,128)(2,1)}), bf16[512,8,32]{0,2,1:T(8,128)(2,1)S(1)}, u32[]{:S(2)}, u32[]{:S(2)}) %all-to-all-start.1) | async-done | bytes 262176 | tf_op jit(solution)/shard_map/all_to_all | solution.py:46
  108.9 0.1 fusion.23
  109.0 0.3 fusion.28
  109.4 0.4 convolution_add_fusion
  109.8 0.0 copy-done.1
  109.8 1.1 fusion.19
  (5 shorter events, 0.1 us)
Async XLA Ops:
  6.5 1.6 %copy-start = (bf16[256,2048]{1,0:T(8,128)(2,1)S(1)}, bf16[256,2048]{1,0:T(8,128)(2,1)}, u32[]{:S(2)}) copy-start(bf16[256,2048]{1,0:T(8,128)(2,1)} %param.9) | copy-start | bytes 3145732
  6.5 44.5 %all-gather.2.cloned.1.call-start = ((), (), s32[]{:S(2)}) async-start(), calls=%async_computation.3 | async-start | bytes 1310720 | tf_op jit(solution)/shard_map/all_gather | solution.py:33
  25.4 69.2 %reduce-scatter.2.cloned.1.call-start = ((), (), s32[]{:S(2)}) async-start(), calls=%async_computation.4 | async-start | bytes 1310720 | tf_op jit(solution)/shard_map/reduce_scatter | solution.py:38
  55.9 7.0 %copy-start.2 = (s32[8,32]{1,0:T(8,128)S(1)}, s32[8,32]{1,0:T(8,128)}, u32[]{:S(2)}) copy-start(s32[8,32]{1,0:T(8,128)} %param.16) | copy-start | bytes 3076
  55.9 7.1 %copy-start.4 = (f32[8,32]{1,0:T(8,128)S(1)}, f32[8,32]{1,0:T(8,128)}, u32[]{:S(2)}) copy-start(f32[8,32]{1,0:T(8,128)} %param.17) | copy-start | bytes 3076
  56.0 7.1 %copy-start.3 = (bf16[2048]{0:T(1024)(128)(2,1)S(1)}, bf16[2048]{0:T(1024)(128)(2,1)}, u32[]{:S(2)}) copy-start(bf16[2048]{0:T(1024)(128)(2,1)} %param.15) | copy-start | bytes 12292
  63.1 46.7 %copy-start.1 = (bf16[1024,512]{1,0:T(8,128)(2,1)S(1)}, bf16[1024,512]{1,0:T(8,128)(2,1)}, u32[]{:S(2)}) copy-start(bf16[1024,512]{1,0:T(8,128)(2,1)} %param.14) | copy-start | bytes 3145732
  94.6 14.3 %all-to-all-start.1 = ((bf16[512,8,32]{0,2,1:T(8,128)(2,1)}), bf16[512,8,32]{0,2,1:T(8,128)(2,1)S(1)}, u32[]{:S(2)}, u32[]{:S(2)}) async-start(bf16[512,8,32]{0,2,1:T(8,128)(2,1)} %bitcast.46), calls=%async_computation.2 | async-start | bytes 524288 | tf_op jit(solution)/shard_map/all_to_all | solution.py:46
Sparse Core Ops, SparseCore 0:
  25.5 25.4 all-gather.1
  63.0 31.4 reduce-scatter.1
